TPU v7x, 128 devices: a whole 4x4x4 slice. The times are simulated.
128 devices in a mesh: sp: 64 (over z, y, x), tp: 2 (over core).
Axes of the slice: x: 4, y: 4, z: 4, core: 2. Of those that a mesh axis runs over, the one named last changes fastest.
Arguments:
- query_matrix: bfloat16 [16384, 2048], P('sp', 'tp'), may hold values from -6 to 6
- key_matrix: bfloat16 [16384, 2048], P('sp', 'tp'), may hold values from -6 to 6
- value_matrix: bfloat16 [16384, 2048], P('sp', 'tp'), may hold values from -6 to 6
- output_gate_logits: bfloat16 [16384, 2048], P('sp', 'tp'), may hold values from -6 to 6
- decay_preactivation: bfloat16 [16384, 2048], P('sp', 'tp'), may hold values from -3 to 12
- head_extra_decay: float32 [16384, 32], P('sp', 'tp'), may hold values from -0.7 to 0
- residual: bfloat16 [16384, 2048], P(('sp', 'tp')), may hold values from -6 to 6
- head_norm_gain: float32 [64], replicated, may hold values from 0.1 to 1.9
- output_projection_weight: bfloat16 [2048, 2048], P('tp'), may hold values from -0.125 to 0.125
- mixer_norm_gain: float32 [2048], replicated, may hold values from 0.1 to 1.9
- routes: int32 [16384, 2], P(('sp', 'tp')), may hold values from 0 to 63, all different within a row; in each aligned block of 128 rows (0 to 127, 128 to 255, ...) at most 8 rows name the same one
- routing_weight: float32 [16384, 2], P(('sp', 'tp')), may hold values from 0.2 to 1.5
- routed_gate_weight: bfloat16 [64, 2048, 1024], P('sp', None, 'tp'), may hold values from -0.125 to 0.125
- routed_up_weight: bfloat16 [64, 2048, 1024], P('sp', None, 'tp'), may hold values from -0.125 to 0.125
- routed_down_weight: bfloat16 [64, 1024, 2048], P('sp', 'tp'), may hold values from -0.1875 to 0.1875
- common_gate_weight: bfloat16 [2048, 512], replicated, may hold values from -0.125 to 0.125
- common_up_weight: bfloat16 [2048, 512], replicated, may hold values from -0.125 to 0.125
- common_down_weight: bfloat16 [512, 2048], replicated, may hold values from -0.25 to 0.25
- final_norm_gain: float32 [2048], replicated, may hold values from 0.1 to 1.9
Outputs:
- layer_out: bfloat16 [16384, 2048], P(('sp', 'tp'))
Inputs may be any that keep to these rules, and one draw needn't show every extreme that they name: `routes`: each row names 2 different experts. In the rows of one device (aligned blocks of rows) no expert is named by more than 8 rows, a bound that some block reaches.
All inputs are finite; a program needn't handle non-finite values.
Results may differ from a plain program's by a relative error of at most 0.019.
Values may be sent and summed in bfloat16 or wider, within the bound.
A program may use at most 192 MiB of HBM per device.

v0:
```python
import jax
import jax.numpy as jnp
from jax import lax
from jax.sharding import Mesh
from jax.sharding import PartitionSpec as P

HEAD_NUMBER = 32
KEY_HEAD_SIZE = 64
BLOCK_TOKENS = 64
SP = ("sp_0", "sp_1", "sp_2")
SP_TP = ("sp_0", "sp_1", "sp_2", "tp")


EPS = 1e-06
GATE_DIVISOR = 16.0


def neutral_like(shard, identity):
    return jax.tree.map(
        lambda part, zero: jnp.zeros_like(part) + jnp.asarray(zero, part.dtype), shard, identity
    )


def entering(shard, axes, combine, identity, reverse):
    before = start = neutral_like(shard, identity)
    running = shard
    for axis in reversed(axes):
        devices, place = (lax.axis_size(axis), lax.axis_index(axis))
        pieces = jax.tree.map(
            lambda part, kind: lax.all_gather(part.astype(kind), axis),
            running,
            (jnp.bfloat16, jnp.bfloat16),
        )
        inside, running = (start, start)
        for k in reversed(range(devices)) if reverse else range(devices):
            passed = k > place if reverse else k < place
            running = combine(
                running, jax.tree.map(lambda part, own: part[k].astype(own.dtype), pieces, shard)
            )
            inside = jax.tree.map(lambda new, old: jnp.where(passed, new, old), running, inside)
        before = combine(inside, before)
    return before


def layer_norm(values, gain):
    center = values - jnp.mean(values, axis=-1, keepdims=True)
    spread = jnp.mean(center * center, axis=-1, keepdims=True)
    return center * lax.rsqrt(spread + EPS) * gain


def carry_combine(earlier, later):
    return (earlier[0] + later[0], jnp.exp(later[0])[..., None] * earlier[1] + later[1])


def block_products(
    query_matrix, key_matrix, value_matrix, decay_preactivation, head_extra_decay, number_of_heads
):
    token_count = query_matrix.shape[0]
    number_of_blocks = token_count // BLOCK_TOKENS
    blocked_layout = (number_of_blocks, BLOCK_TOKENS, number_of_heads, KEY_HEAD_SIZE)
    logarithm_decay = jax.nn.log_sigmoid(decay_preactivation.astype(jnp.float32)).reshape(
        token_count, number_of_heads, KEY_HEAD_SIZE
    )
    logarithm_decay = (logarithm_decay / GATE_DIVISOR + head_extra_decay[:, :, None]).reshape(
        blocked_layout
    )
    inside_block = jnp.cumsum(logarithm_decay, axis=1)
    block_total = inside_block[:, -1]
    query_float = query_matrix.astype(jnp.float32).reshape(blocked_layout) * KEY_HEAD_SIZE ** (-0.5)
    key_float = key_matrix.astype(jnp.float32).reshape(blocked_layout)
    value_f = value_matrix.astype(jnp.float32).reshape(blocked_layout)
    query_up = query_float * jnp.exp(inside_block)
    query_down = query_float * jnp.exp(-inside_block)
    key_up = key_float * jnp.exp(inside_block)
    key_down = key_float * jnp.exp(-inside_block)
    lower_mask = jnp.tril(jnp.ones((BLOCK_TOKENS, BLOCK_TOKENS), bool))
    ahead = jnp.einsum("nihc,njhc->nhij", query_up, key_down)
    behind = jnp.einsum("nihc,njhc->nhij", query_down, key_up)
    scores = jnp.where(lower_mask, ahead, 0.0) + jnp.where(lower_mask, 0.0, behind)
    local_out = jnp.einsum("nhij,njhv->nihv", scores, value_f)
    key_end = key_float * jnp.exp(block_total[:, None] - inside_block)
    left_sum = jnp.einsum("njhc,njhv->nhcv", key_end, value_f)
    right_sum = jnp.einsum("njhc,njhv->nhcv", key_up, value_f)

    def carry_step(carried, fragments):
        total, summed = fragments
        return (jnp.exp(total)[..., None] * carried + summed, carried)

    zero_state = jnp.zeros(left_sum.shape[1:], jnp.float32)
    left_dev, left_before = lax.scan(carry_step, zero_state, (block_total, left_sum))
    right_dev, right_after = lax.scan(
        carry_step, zero_state, (block_total, right_sum), reverse=True
    )
    query_tail = query_float * jnp.exp(block_total[:, None] - inside_block)
    local_out = local_out + jnp.einsum("nihc,nhcv->nihv", query_up, left_before)
    local_out = local_out + jnp.einsum("nihc,nhcv->nihv", query_tail, right_after)
    before_blocks = jnp.cumsum(block_total, axis=0) - block_total
    device_total = jnp.sum(block_total, axis=0)
    from_start = inside_block + before_blocks[:, None]
    query_head = query_float * jnp.exp(from_start)
    query_rest = query_float * jnp.exp(device_total[None, None] - from_start)
    return (local_out, query_head, query_rest, device_total, left_dev, right_dev)


def expert_half(arrived, gate_half, up_half, down_half):
    flat_rows = arrived.reshape(-1, arrived.shape[-1])
    gate_part = jnp.dot(flat_rows, gate_half, preferred_element_type=jnp.float32)
    up_part = jnp.dot(flat_rows, up_half, preferred_element_type=jnp.float32)
    inner = (jax.nn.silu(gate_part) * up_part).astype(jnp.bfloat16)
    partial_out = jnp.dot(inner, down_half, preferred_element_type=jnp.float32).astype(jnp.bfloat16)
    return partial_out.reshape(arrived.shape)


def per_device(
    query_matrix,
    key_matrix,
    value_matrix,
    output_gate_logits,
    decay_preactivation,
    head_extra_decay,
    residual,
    head_norm_gain,
    output_projection_weight,
    mixer_norm_gain,
    routes,
    routing_weight,
    routed_gate_weight,
    routed_up_weight,
    routed_down_weight,
    common_gate_weight,
    common_up_weight,
    common_down_weight,
    final_norm_gain,
):
    tp_size = lax.axis_size("tp")
    number_of_heads = HEAD_NUMBER // tp_size
    token_count = query_matrix.shape[0]
    local_out, query_head, query_rest, device_total, left_dev, right_dev = block_products(
        query_matrix,
        key_matrix,
        value_matrix,
        decay_preactivation,
        head_extra_decay,
        number_of_heads,
    )
    identity = (jnp.zeros_like(device_total), jnp.zeros_like(left_dev))
    left_in = entering((device_total, left_dev), SP, carry_combine, identity, False)[1]
    right_in = entering((device_total, right_dev), SP, carry_combine, identity, True)[1]
    mixed = local_out + jnp.einsum("nihc,hcv->nihv", query_head, left_in)
    mixed = mixed + jnp.einsum("nihc,hcv->nihv", query_rest, right_in)
    mixed = mixed.reshape(token_count, number_of_heads, KEY_HEAD_SIZE)
    normed_heads = (
        mixed * lax.rsqrt(jnp.mean(mixed * mixed, axis=-1, keepdims=True) + EPS) * head_norm_gain
    )
    gated = (
        normed_heads.reshape(token_count, number_of_heads * KEY_HEAD_SIZE)
        * jax.nn.silu(output_gate_logits.astype(jnp.float32))
    ).astype(jnp.bfloat16)
    projected = lax.psum_scatter(
        jnp.dot(gated, output_projection_weight, preferred_element_type=jnp.float32).astype(
            jnp.bfloat16
        ),
        "tp",
        scatter_dimension=0,
        tiled=True,
    ).astype(jnp.float32)
    normed = layer_norm(residual.astype(jnp.float32) + projected, mixer_norm_gain).astype(
        jnp.bfloat16
    )
    row_count = normed.shape[0]
    model_width = normed.shape[1]
    top_count = routes.shape[1]
    experts = lax.axis_size(SP)
    capacity = max(2, row_count * top_count // experts * 2)
    flat_expert = routes.reshape(-1)
    member = (flat_expert[:, None] == jnp.arange(experts, dtype=jnp.int32)[None, :]).astype(
        jnp.int32
    )
    rank_in = jnp.sum((jnp.cumsum(member, axis=0) - member) * member, axis=1)
    slot_of = flat_expert * capacity + rank_in
    source_row = (
        jnp.zeros((experts * capacity,), jnp.int32)
        .at[slot_of]
        .set(jnp.arange(row_count * top_count, dtype=jnp.int32) // top_count)
    )
    outbound = normed[source_row].reshape(experts, capacity, model_width)
    gate_half = routed_gate_weight[0]
    up_half = routed_up_weight[0]
    down_half = routed_down_weight[0]
    paired = lax.all_gather(
        lax.all_to_all(outbound, SP, split_axis=0, concat_axis=0, tiled=True),
        "tp",
        axis=0,
        tiled=True,
    )
    partial_out = expert_half(paired, gate_half, up_half, down_half).astype(jnp.float32)
    summed = lax.psum_scatter(
        partial_out.astype(jnp.bfloat16), "tp", scatter_dimension=0, tiled=True
    )
    expert_out = lax.all_to_all(summed, SP, split_axis=0, concat_axis=0, tiled=True)
    flat_out = expert_out.reshape(experts * capacity, model_width)
    picked = flat_out[slot_of].astype(jnp.float32).reshape(row_count, top_count, model_width)
    routed = jnp.einsum("rk,rkd->rd", routing_weight, picked)
    shared_gate_out = jnp.dot(normed, common_gate_weight, preferred_element_type=jnp.float32)
    shared_up_out = jnp.dot(normed, common_up_weight, preferred_element_type=jnp.float32)
    shared_inner = (jax.nn.silu(shared_gate_out) * shared_up_out).astype(jnp.bfloat16)
    feed = jnp.dot(shared_inner, common_down_weight, preferred_element_type=jnp.float32) + routed
    return layer_norm(normed.astype(jnp.float32) + feed, final_norm_gain).astype(jnp.bfloat16)


def solution(mesh):
    torus = Mesh(mesh.devices.reshape(4, 4, 4, mesh.shape["tp"]), ("sp_0", "sp_1", "sp_2", "tp"))
    return jax.shard_map(
        per_device,
        mesh=torus,
        in_specs=(
            P(SP, "tp"),
            P(SP, "tp"),
            P(SP, "tp"),
            P(SP, "tp"),
            P(SP, "tp"),
            P(SP, "tp"),
            P(SP_TP, None),
            P(),
            P("tp", None),
            P(),
            P(SP_TP, None),
            P(SP_TP, None),
            P(SP, None, "tp"),
            P(SP, None, "tp"),
            P(SP, "tp", None),
            P(),
            P(),
            P(),
            P(),
        ),
        out_specs=P(SP_TP, None),
        check_vma=False,
    )
```

profile of v0, /device:TPU:1, one launch (start us, length us, event | category | flops | bytes accessed | tf_op | source)
XLA Modules:
  0.0 414.3 jit_solution(4577545458539700706)
XLA Ops:
  13.8 10.3 %all-gather = bf16[64,64]{1,0:T(8,128)(2,1)S(1)} all-gather(bf16[16,64]{1,0:T(8,128)(2,1)S(1)} %convert_element_type.566), channel_id=2, replica_groups=mesh['sp_0'=4,'sp_1'=4,'sp_2'=4,'tp'=2] {'sp_2'}, dimensions={0}, use_global_device_ids=true | all-gather | bytes 10240 | tf_op jit(solution)/shard_map/all_gather | solution.py:30
  24.1 9.6 %all_gather.54 = bf16[4,16,64]{2,1,0:T(8,128)(2,1)S(1)} all-gather(bf16[1,16,64]{2,1,0:T(8,128)(2,1)S(1)} %get-tuple-element.230), channel_id=1, replica_groups=mesh['sp_0'=4,'sp_1'=4,'sp_2'=4,'tp'=2] {'sp_1'}, dimensions={0}, use_global_device_ids=true | all-gather | bytes 10240 | tf_op jit(solution)/shard_map/all_gather | solution.py:30
  41.5 5.9 %exponential_multiply_fusion.1 = (bf16[4,64,16,64]{3,2,1,0:T(8,128)(2,1)}, bf16[4,64,16,64]{3,2,1,0:T(8,128)(2,1)}, bf16[4,64,16,64]{3,2,1,0:T(8,128)(2,1)}, bf1...) fusion(f32[4,64,16,64]{3,2,1,0:T(8,128)} %mul.472, ...), kind=kLoop, calls=%fused_computation.40 | loop fusion | flops 5242880 | bytes 7376896 | tf_op jit(solution)/shard_map/mul | solution.py:100
  57.2 8.5 %while.31 = (s32[]{:T(128)}, f32[16,64,64]{2,1,0:T(8,128)S(1)}, bf16[4,16,64,64]{3,2,1,0:T(8,128)(2,1)}, f32[4,16,64]{2,1,0:T(8,128)S(1)}, f32[4,16,64,64]{3,2,1,0:T(8,128)}, /*index=5*/s32[]{:T(128)}, s32[]{:T(128)}, s32[]{:T(128)}) while((s32[]{:T(128)}, f32[16,64,64]{2,1,0:T(8,128)S(1)}, bf16[4,16,64,64]{3,2,1,0:T(8,128)(2,1)}, ...), condition=%wide.region_4.5_spmd.clone, body=%wide.region_3.4_spmd.clone.sunk | while | flops 262148 | bytes 1323128 | solution.py:91
  65.7 12.5 %all-gather.2 = bf16[64,64,64]{2,1,0:T(8,128)(2,1)} all-gather(bf16[16,64,64]{2,1,0:T(8,128)(2,1)S(1)} %convert_element_type.635), channel_id=4, replica_groups=mesh['sp_0'=4,'sp_1'=4,'sp_2'=4,'tp'=2] {'sp_2'}, dimensions={0}, use_global_device_ids=true | all-gather | bytes 655360 | tf_op jit(solution)/shard_map/all_gather | solution.py:30
  81.5 8.5 %while.30 = (s32[]{:T(128)}, f32[16,64,64]{2,1,0:T(8,128)S(1)}, bf16[4,16,64,64]{3,2,1,0:T(8,128)(2,1)}, f32[4,16,64]{2,1,0:T(8,128)S(1)}, f32[4,16,64,64]{3,2,1,0:T(8,128)}, /*index=5*/s32[]{:T(128)}, s32[]{:T(128)}) while((s32[]{:T(128)}, f32[16,64,64]{2,1,0:T(8,128)S(1)}, bf16[4,16,64,64]{3,2,1,0:T(8,128)(2,1)}, ...), condition=%wide.region_2.3_spmd.clone, body=%wide.region_1.2_spmd.clone.sunk | while | flops 262147 | bytes 1323616 | solution.py:90
  90.0 11.1 %all-gather.1 = bf16[64,64,64]{2,1,0:T(8,128)(2,1)S(1)} all-gather(bf16[16,64,64]{2,1,0:T(8,128)(2,1)S(1)} %convert_element_type.590), channel_id=3, replica_groups=mesh['sp_0'=4,'sp_1'=4,'sp_2'=4,'tp'=2] {'sp_2'}, dimensions={0}, use_global_device_ids=true | all-gather | bytes 655360 | tf_op jit(solution)/shard_map/all_gather | solution.py:30
  102.2 11.2 %all_gather.58 = bf16[4,16,64,64]{3,2,1,0:T(8,128)(2,1)S(1)} all-gather(bf16[1,16,64,64]{3,2,1,0:T(8,128)(2,1)S(1)} %get-tuple-element.228), channel_id=1, replica_groups=mesh['sp_0'=4,'sp_1'=4,'sp_2'=4,'tp'=2] {'sp_1'}, dimensions={0}, use_global_device_ids=true | all-gather | bytes 655360 | tf_op jit(solution)/shard_map/all_gather | solution.py:30
  114.1 13.3 %all_gather.59 = bf16[4,16,64,64]{3,2,1,0:T(8,128)(2,1)} all-gather(bf16[1,16,64,64]{3,2,1,0:T(8,128)(2,1)S(1)} %fusion.103), channel_id=1, replica_groups=mesh['sp_0'=4,'sp_1'=4,'sp_2'=4,'tp'=2] {'sp_0'}, dimensions={0}, use_global_device_ids=true | all-gather | bytes 655360 | tf_op jit(solution)/shard_map/all_gather | solution.py:30
  127.4 9.3 %all_gather.55 = bf16[4,16,64]{2,1,0:T(8,128)(2,1)S(1)} all-gather(bf16[1,16,64]{2,1,0:T(8,128)(2,1)S(1)} %get-tuple-element.218), channel_id=1, replica_groups=mesh['sp_0'=4,'sp_1'=4,'sp_2'=4,'tp'=2] {'sp_0'}, dimensions={0}, use_global_device_ids=true | all-gather | bytes 10240 | tf_op jit(solution)/shard_map/all_gather | solution.py:30
  136.7 11.4 %all_gather.64 = bf16[4,16,64,64]{3,2,1,0:T(8,128)(2,1)S(1)} all-gather(bf16[1,16,64,64]{3,2,1,0:T(8,128)(2,1)S(1)} %get-tuple-element.229), channel_id=1, replica_groups=mesh['sp_0'=4,'sp_1'=4,'sp_2'=4,'tp'=2] {'sp_1'}, dimensions={0}, use_global_device_ids=true | all-gather | bytes 655360 | tf_op jit(solution)/shard_map/all_gather | solution.py:30
  148.2 9.1 %all_gather.60 = bf16[4,16,64]{2,1,0:T(8,128)(2,1)S(1)} all-gather(bf16[1,16,64]{2,1,0:T(8,128)(2,1)S(1)} %get-tuple-element.231), channel_id=1, replica_groups=mesh['sp_0'=4,'sp_1'=4,'sp_2'=4,'tp'=2] {'sp_1'}, dimensions={0}, use_global_device_ids=true | all-gather | bytes 10240 | tf_op jit(solution)/shard_map/all_gather | solution.py:30
  158.0 12.2 %all_gather.65 = bf16[4,16,64,64]{3,2,1,0:T(8,128)(2,1)} all-gather(bf16[1,16,64,64]{3,2,1,0:T(8,128)(2,1)S(1)} %fusion.121), channel_id=1, replica_groups=mesh['sp_0'=4,'sp_1'=4,'sp_2'=4,'tp'=2] {'sp_0'}, dimensions={0}, use_global_device_ids=true | all-gather | bytes 655360 | tf_op jit(solution)/shard_map/all_gather | solution.py:30
  170.2 9.3 %all_gather.61 = bf16[4,16,64]{2,1,0:T(8,128)(2,1)S(1)} all-gather(bf16[1,16,64]{2,1,0:T(8,128)(2,1)S(1)} %get-tuple-element.236), channel_id=1, replica_groups=mesh['sp_0'=4,'sp_1'=4,'sp_2'=4,'tp'=2] {'sp_0'}, dimensions={0}, use_global_device_ids=true | all-gather | bytes 10240 | tf_op jit(solution)/shard_map/all_gather | solution.py:30
  193.6 5.5 %fusion.8 = f32[16,64,4,64]{3,1,0,2:T(8,128)S(1)} fusion(bf16[4,64,16,64]{3,2,1,0:T(8,128)(2,1)S(1)} %copy-done.19, bf16[4,16,64,64]{3,2,1,0:T(8,128)(2,1)} %all_gather.65, f32[16,64]{1,0:T(8,128)S(1)} %get-tuple-element.211, f32[16,64]{1,0:T(8,128)S(1)} %get-tuple-element.227, f32[16,64]{1,0:T(8,128)S(1)} %get-tuple-element.240, ...), kind=kOutput, calls=%fused_computation.25 | convolution fusion | flops 36765696 | bytes 3203084 | tf_op jit(solution)/shard_map/nihc,hcv->nihv/dot_general | solution.py:150
  208.9 5.4 %convolution_convert_fusion = bf16[256,2048]{1,0:T(8,128)(2,1)} fusion(bf16[1024,2048]{1,0:T(8,128)(2,1)} %param.31, bf16[256,1024]{1,0:T(8,128)(2,1)} %param.26, f32[256,1024]{1,0:T(8,128)} %reshape.507, f32[256,1024]{1,0:T(8,128)} %copy.102, f32[1024]{0:T(1024)S(1)} %mul.570), kind=kOutput, calls=%fused_computation.15 | convolution fusion | flops 1076625408 | bytes 7868416 | tf_op jit(solution)/shard_map/dot_general | solution.py:160
  217.5 38.2 %reduce-scatter.3.cloned.1.call-done = bf16[128,2048]{1,0:T(8,128)(2,1)} async-done(((bf16[256,2048]{1,0:T(8,128)(2,1)}), bf16[128,2048]{1,0:T(8,128)(2,1)}) %reduce-scatter.3.cloned.1.call-update) | async-done | bytes 524304 | tf_op jit(solution)/shard_map/reduce_scatter | solution.py:159
  262.0 39.3 %all_to_all.10 = bf16[64,8,2048]{2,1,0:T(8,128)(2,1)} all-to-all(bf16[64,8,2048]{2,1,0:T(8,128)(2,1)} %bitcast.432), channel_id=1, replica_groups=mesh['sp_0'=4,'sp_1'=4,'sp_2'=4,'tp'=2] {'sp_0','sp_1','sp_2'}, dimensions={0} | all-to-all | bytes 4194304 | tf_op jit(solution)/shard_map/all_to_all | solution.py:191
  301.4 14.8 %all-gather.5.cloned.1.call-done = bf16[128,8,2048]{2,1,0:T(8,128)(2,1)} async-done(((bf16[64,8,2048]{2,1,0:T(8,128)(2,1)}), bf16[128,8,2048]{2,1,0:T(8,128)(2,1)}) %all-gather.5.cloned.1.call-update) | async-done | bytes 4194320 | tf_op jit(solution)/shard_map/all_gather | solution.py:190
  316.2 6.5 %fusion.2 = f32[1024,512]{1,0:T(8,128)} fusion(bf16[128,8,2048]{2,1,0:T(8,128)(2,1)} %all-gather.5.cloned.1.call-done, bf16[1,2048,512]{2,1,0:T(8,128)(2,1)} %param.35), kind=kOutput, calls=%fused_computation.11 | convolution fusion | flops 2147483648 | bytes 8388608 | tf_op jit(solution)/shard_map/dot_general | solution.py:107
  322.7 10.0 %convert_bitcast_fusion = bf16[128,8,2048]{2,1,0:T(8,128)(2,1)} fusion(bf16[1,512,2048]{2,1,0:T(8,128)(2,1)S(1)} %copy-done, f32[1024,512]{1,0:T(8,128)} %fusion.2, bf16[1,2048,512]{2,1,0:T(8,128)(2,1)} %param.36, bf16[128,8,2048]{2,1,0:T(8,128)(2,1)} %all-gather.5.cloned.1.call-done), kind=kOutput, calls=%fused_computation.13 | convolution fusion | flops 4300210176 | bytes 14680064 | tf_op jit(solution)/shard_map/dot_general | solution.py:110
  332.8 16.2 %reduce-scatter.5.cloned.1.call-done = bf16[64,8,2048]{2,1,0:T(8,128)(2,1)} async-done(((bf16[128,8,2048]{2,1,0:T(8,128)(2,1)}), bf16[64,8,2048]{2,1,0:T(8,128)(2,1)}) %reduce-scatter.5.cloned.1.call-update) | async-done | bytes 2097168 | tf_op jit(solution)/shard_map/reduce_scatter | solution.py:197
  349.0 10.4 %all-to-all-start.1 = ((bf16[64,8,2048]{2,1,0:T(8,128)(2,1)}), bf16[64,8,2048]{2,1,0:T(8,128)(2,1)}, u32[]{:S(2)}, u32[]{:S(2)}) async-start(bf16[64,8,2048]{2,1,0:T(8,128)(2,1)} %reduce-scatter.5.cloned.1.call-done), calls=%async_computation.3 | async-start | bytes 4194304 | tf_op jit(solution)/shard_map/all_to_all | solution.py:200
  361.6 26.6 %all-to-all-done.1 = bf16[64,8,2048]{2,1,0:T(8,128)(2,1)} async-done(((bf16[64,8,2048]{2,1,0:T(8,128)(2,1)}), bf16[64,8,2048]{2,1,0:T(8,128)(2,1)}, u32[]{:S(2)}, u32[]{:S(2)}) %all-to-all-start.1) | async-done | bytes 2097184 | tf_op jit(solution)/shard_map/all_to_all | solution.py:200
  (162 shorter events, 102.2 us)
Async XLA Ops:
  6.5 316.2 %copy-start = (bf16[1,512,2048]{2,1,0:T(8,128)(2,1)S(1)}, bf16[1,512,2048]{2,1,0:T(8,128)(2,1)}, u32[]{:S(2)}) copy-start(bf16[1,512,2048]{2,1,0:T(8,128)(2,1)} %param.37) | copy-start | bytes 6291460
  6.5 249.2 %reduce-scatter.3.cloned.1.call-start = ((), (), s32[]{:S(2)}) async-start(), calls=%async_computation.4 | async-start | bytes 1572864 | tf_op jit(solution)/shard_map/reduce_scatter | solution.py:159
  6.5 3.8 copy-start.20
  65.7 12.6 %copy-start.1 = (bf16[4,64,16,64]{3,2,1,0:T(8,128)(2,1)S(1)}, bf16[4,64,16,64]{3,2,1,0:T(8,128)(2,1)}, u32[]{:S(2)}) copy-start(bf16[4,64,16,64]{3,2,1,0:T(8,128)(2,1)} %reshape.506) | copy-start | bytes 1572868
  65.7 12.6 %copy-start.15 = (bf16[4,64,16,64]{3,2,1,0:T(8,128)(2,1)S(1)}, bf16[4,64,16,64]{3,2,1,0:T(8,128)(2,1)}, u32[]{:S(2)}) copy-start(bf16[4,64,16,64]{3,2,1,0:T(8,128)(2,1)} %get-tuple-element.206) | copy-start | bytes 1572868
  89.9 11.2 %copy-start.16 = (bf16[64,64,64]{2,1,0:T(8,128)(2,1)S(1)}, bf16[64,64,64]{2,1,0:T(8,128)(2,1)}, u32[]{:S(2)}) copy-start(bf16[64,64,64]{2,1,0:T(8,128)(2,1)} %all-gather.2) | copy-start | bytes 1572868
  101.1 13.1 %copy-start.17 = (bf16[64,64,64]{2,1,0:T(8,128)(2,1)}, bf16[64,64,64]{2,1,0:T(8,128)(2,1)S(1)}, u32[]{:S(2)}) copy-start(bf16[64,64,64]{2,1,0:T(8,128)(2,1)S(1)} %all-gather.1) | copy-start | bytes 1572868
  113.4 23.3 %copy-start.12 = (bf16[4,16,64,64]{3,2,1,0:T(8,128)(2,1)}, bf16[4,16,64,64]{3,2,1,0:T(8,128)(2,1)S(1)}, u32[]{:S(2)}) copy-start(bf16[4,16,64,64]{3,2,1,0:T(8,128)(2,1)S(1)} %all_gather.58) | copy-start | bytes 1572868
  127.4 52.1 %copy-start.4 = (bf16[4,64,16,64]{1,3,2,0:T(8,128)(2,1)S(1)}, bf16[4,64,16,64]{1,3,2,0:T(8,128)(2,1)}, u32[]{:S(2)}) copy-start(bf16[4,64,16,64]{1,3,2,0:T(8,128)(2,1)} %copy.92) | copy-start | bytes 1572868
  127.4 52.1 %copy-start.14 = (bf16[4,64,16,64]{3,2,1,0:T(8,128)(2,1)S(1)}, bf16[4,64,16,64]{3,2,1,0:T(8,128)(2,1)}, u32[]{:S(2)}) copy-start(bf16[4,64,16,64]{3,2,1,0:T(8,128)(2,1)} %get-tuple-element.203) | copy-start | bytes 1572868
  148.2 9.1 %copy-start.11 = (bf16[4,16,64,64]{3,2,1,0:T(8,128)(2,1)}, bf16[4,16,64,64]{3,2,1,0:T(8,128)(2,1)S(1)}, u32[]{:S(2)}) copy-start(bf16[4,16,64,64]{3,2,1,0:T(8,128)(2,1)S(1)} %all_gather.64) | copy-start | bytes 1572868
  188.5 5.0 %copy-start.19 = (bf16[4,64,16,64]{3,2,1,0:T(8,128)(2,1)S(1)}, bf16[4,64,16,64]{3,2,1,0:T(8,128)(2,1)}, u32[]{:S(2)}) copy-start(bf16[4,64,16,64]{3,2,1,0:T(8,128)(2,1)} %get-tuple-element.198) | copy-start | bytes 1572868
  193.5 5.6 %copy-start.3 = (bf16[4,64,16,64]{3,2,1,0:T(8,128)(2,1)S(1)}, bf16[4,64,16,64]{3,2,1,0:T(8,128)(2,1)}, u32[]{:S(2)}) copy-start(bf16[4,64,16,64]{3,2,1,0:T(8,128)(2,1)} %get-tuple-element.199) | copy-start | bytes 1572868
  193.5 5.6 %copy-start.6 = (f32[4,16,64,64]{3,2,1,0:T(8,128)S(1)}, f32[4,16,64,64]{3,2,1,0:T(8,128)}, u32[]{:S(2)}) copy-start(f32[4,16,64,64]{3,2,1,0:T(8,128)} %fusion.12) | copy-start | bytes 3145732
  193.5 5.6 %copy-start.7 = (f32[4,16,64,64]{2,3,1,0:T(8,128)S(1)}, f32[4,16,64,64]{2,3,1,0:T(8,128)}, u32[]{:S(2)}) copy-start(f32[4,16,64,64]{2,3,1,0:T(8,128)} %fusion.20) | copy-start | bytes 3145732
  193.6 5.6 %copy-start.10 = (bf16[4,16,64,64]{3,2,1,0:T(8,128)(2,1)S(1)}, bf16[4,16,64,64]{3,2,1,0:T(8,128)(2,1)}, u32[]{:S(2)}) copy-start(bf16[4,16,64,64]{3,2,1,0:T(8,128)(2,1)} %get-tuple-element.137) | copy-start | bytes 1572868
  208.9 5.5 %copy-start.23 = (s32[128,2]{0,1:T(2,128)S(1)}, s32[128,2]{0,1:T(2,128)}, u32[]{:S(2)}) copy-start(s32[128,2]{0,1:T(2,128)} %param.33) | copy-start | bytes 3076
  214.4 41.3 %copy-start.8 = (bf16[128,2048]{1,0:T(8,128)(2,1)S(1)}, bf16[128,2048]{1,0:T(8,128)(2,1)}, u32[]{:S(2)}) copy-start(bf16[128,2048]{1,0:T(8,128)(2,1)} %param.29) | copy-start | bytes 1572868
  214.4 44.0 %copy-start.21 = (f32[2048]{0:T(1024)S(1)}, f32[2048]{0:T(1024)}, u32[]{:S(2)}) copy-start(f32[2048]{0:T(1024)} %param.32) | copy-start | bytes 24580
  214.4 101.8 %all-gather.5.cloned.1.call-start = ((), (), s32[]{:S(2)}) async-start(), calls=%async_computation.5 | async-start | bytes 6291456 | tf_op jit(solution)/shard_map/all_gather | solution.py:190
  301.4 47.6 %reduce-scatter.5.cloned.1.call-start = ((), (), s32[]{:S(2)}) async-start(), calls=%async_computation.6 | async-start | bytes 6291456 | tf_op jit(solution)/shard_map/reduce_scatter | solution.py:197
  332.8 26.6 %copy-start.24 = (f32[128,2]{0,1:T(2,128)S(1)}, f32[128,2]{0,1:T(2,128)}, u32[]{:S(2)}) copy-start(f32[128,2]{0,1:T(2,128)} %param.34) | copy-start | bytes 3076
  349.0 39.3 %all-to-all-start.1 = ((bf16[64,8,2048]{2,1,0:T(8,128)(2,1)}), bf16[64,8,2048]{2,1,0:T(8,128)(2,1)}, u32[]{:S(2)}, u32[]{:S(2)}) async-start(bf16[64,8,2048]{2,1,0:T(8,128)(2,1)} %reduce-scatter.5.cloned.1.call-done), calls=%async_computation.3 | async-start | bytes 4194304 | tf_op jit(solution)/shard_map/all_to_all | solution.py:200
  399.4 6.1 %copy-start.22 = (f32[2048]{0:T(1024)S(1)}, f32[2048]{0:T(1024)}, u32[]{:S(2)}) copy-start(f32[2048]{0:T(1024)} %param.41) | copy-start | bytes 24580
  (6 other events, 11.4 us)
Sparse Core Ops, SparseCore 0:
  214.5 41.1 reduce-scatter.2
  301.5 14.6 all-gather.4
  332.9 16.0 reduce-scatter.4
where the time goes:
time: 416 us; the launch traced here: 414 us
  blocking collectives  159 us (38%)
  waiting for transfers between devices  95.8 us (23%)
  matrix products  59 us (14%)
  other arithmetic  38.8 us (9%)
  local copies, waits for them, and re-layouts  37.7 us (9%)
  between operations  13.6 us (3%)
  starting transfers between devices  10.5 us (3%)
    all_gather x11, blocking collectives, entering(): lax.all_gather(part.astype(kind), axis)  119 us
    all_to_all x1, blocking collectives, per_device(): lax.all_to_all(outbound, SP, split_axis=0, concat_axis=0, tiled=True)  39.3 us
    reduce_scatter x1, waiting for transfers between devices, per_device(): lax.psum_scatter(jnp.dot(gated, output_projection_weight, preferred_eleme...  38.2 us
    all_to_all x1, waiting for transfers between devices, per_device(): lax.all_to_all(summed, SP, split_axis=0, concat_axis=0, tiled=True)  26.6 us
    reduce_scatter x1, waiting for transfers between devices, per_device(): lax.psum_scatter(partial_out.astype(jnp.bfloat16), 'tp', scatter_dimensio...  16.2 us
    all_gather x1, waiting for transfers between devices, per_device(): lax.all_gather(lax.all_to_all(outbound, SP, split_axis=0, concat_axis=0,...  14.8 us
    add x8, other arithmetic, carry_step(): return (jnp.exp(total)[..., None] * carried + summed, carried)  10.7 us
    all_to_all x1, starting transfers between devices, per_device(): lax.all_to_all(summed, SP, split_axis=0, concat_axis=0, tiled=True)  10.4 us
  transfers between devices with their start and end apart: 4, of which 4 were waited for; matrix products, arithmetic and copies ran while one was open for 1% of the time, Pallas kernels for 0%

commit v1 on v0

v1 whole, which is shorter than its diff:
```python
import jax
import jax.numpy as jnp
from jax import lax
from jax.experimental import pallas as pl
from jax.experimental.pallas import tpu as pltpu
from jax.sharding import PartitionSpec as P

F32 = jnp.float32
BF16 = jnp.bfloat16
MESH = pl.DeviceIdType.MESH
EPS = 1e-06
SP_TP = ("sp", "tp")

N_SP = 64
TOK = 256
ROWS = 128
PAIRS = 8
WIDE = 2048
CHUNKS = 4
PER = N_SP // CHUNKS
CAP = 8
MIX = 27


def dot(a, b):
    return jnp.dot(a, b, preferred_element_type=F32)


def dot_nt(a, b):
    return lax.dot_general(a, b, (((1,), (1,)), ((), ())), preferred_element_type=F32)


def dot_tn(a, b):
    return lax.dot_general(a, b, (((0,), (0,)), ((), ())), preferred_element_type=F32)


def split3(x):
    hi = x.astype(BF16)
    rest = x - hi.astype(F32)
    mid = rest.astype(BF16)
    return hi, mid, (rest - mid.astype(F32)).astype(BF16)


def offset_of(i):
    return (i * MIX) & (N_SP - 1)


def shifted(me, s, sign):
    z = ((me >> 4) + sign * (s >> 4)) & 3
    y = (((me >> 2) & 3) + sign * ((s >> 2) & 3)) & 3
    x = ((me & 3) + sign * (s & 3)) & 3
    return z * 16 + y * 4 + x


def silu(x):
    return x / (1.0 + jnp.exp(-x))


def log_sigmoid(x):
    t = jnp.exp(-jnp.abs(x))
    return jnp.minimum(x, 0.0) - jnp.log1p(t)


def lanes(p, width=128):
    return pl.ds(pl.multiple_of(p * width, width), width)


def iota(shape, axis):
    return lax.broadcasted_iota(jnp.int32, shape, axis)


def layer_kernel(
    q_hbm, k_hbm, v_hbm, g_hbm, a_hbm, x_hbm, res_hbm, hgain_ref, wo_hbm, mgain_ref,
    routes_ref, rw_ref, wg_hbm, wu_hbm, wd_hbm, cg_hbm, cu_hbm, cd_hbm, fgain_ref,
    out_ref,
    q_s, k_s, v_s, g_s, a_s, x_s, res_s, wo_s, cg_s, cu_s, cd_s, wg_s, wu_s, wd_s,
    from_s, local_s, qcat_s, st_out, st_in, tot_out, tot_in, sc_out, inc_s,
    gated_s, own_s, pr_out, pr_in, normed_s, pick_s, comb_s,
    dsp_out, dsp_in, xb_s, inner_s, e_out, ret_s, acc_s,
    ld_sem, w_own_sem, w_send, w_recv, st_send, st_recv, tt_send, tt_recv, sc_send, sc_recv,
    pr_send, pr_recv, d_send, d_recv, r_send, r_recv,
):
    me = lax.axis_index("sp")
    core = lax.axis_index("tp")
    other = 1 - core

    sources = (a_hbm, x_hbm, k_hbm, v_hbm, q_hbm, g_hbm, wo_hbm, res_hbm, cg_hbm, cu_hbm, cd_hbm)
    targets = (a_s, x_s, k_s, v_s, q_s, g_s, wo_s, res_s, cg_s, cu_s, cd_s)
    loads = [
        pltpu.make_async_copy(s, t, ld_sem.at[i]) for i, (s, t) in enumerate(zip(sources, targets))
    ]
    for load in loads[:6]:
        load.start()

    barrier = pltpu.get_barrier_semaphore()

    def greet(s, carry):
        pl.semaphore_signal(
            barrier, inc=1, device_id={"sp": shifted(me, s, 1)}, device_id_type=MESH
        )
        return carry

    lax.fori_loop(1, N_SP, greet, 0)
    pl.semaphore_signal(barrier, inc=1, device_id={"tp": other}, device_id_type=MESH)

    low = iota((TOK, TOK), 0) >= iota((TOK, TOK), 1)
    low_bf = jnp.where(low, 1.0, 0.0).astype(BF16)
    half64 = iota((64, 128), 1) < 64
    for load in loads[:4]:
        load.wait()

    def own_state(p, carry):
        decay = log_sigmoid(a_s[:, lanes(p)].astype(F32)) * (1.0 / 16.0)
        spread = jnp.where(iota((16, 128), 0) == 2 * p + (iota((16, 128), 1) >> 6), 1.0, 0.0)
        spread = spread.astype(BF16)
        for part in split3(x_s[...]):
            decay = decay + dot(part, spread)
        hi, mid, lo = split3(decay)
        total = dot(low_bf, hi) + dot(low_bf, mid) + dot(low_bf, lo)
        from_s[:, lanes(p)] = total
        last = total[TOK - 1 :, :]
        tot_out[p] = jnp.exp(last)
        key = k_s[:, lanes(p)].astype(F32)
        up = (key * jnp.exp(total)).astype(BF16)
        end = (key * jnp.exp(last - total)).astype(BF16)
        value = v_s[:, lanes(p)]
        left = dot_tn(value, end)
        right = dot_tn(value, up)
        left = jnp.where(half64, left[:64], left[64:]).astype(BF16)
        right = jnp.where(half64, right[:64], right[64:]).astype(BF16)
        for part in range(4):
            st_out[4 * p + part] = left[16 * part : 16 * part + 16]
            st_out[32 + 4 * p + part] = right[16 * part : 16 * part + 16]
        return carry

    lax.fori_loop(0, PAIRS, own_state, 0)

    pl.semaphore_wait(barrier, N_SP)

    def send_state(i, carry):
        to = shifted(me, offset_of(i), 1)
        pltpu.make_async_remote_copy(
            st_out.at[to], st_in.at[me], st_send, st_recv,
            device_id={"sp": to}, device_id_type=MESH,
        ).start()
        pltpu.make_async_remote_copy(
            tot_out.at[(to & 31) >> 2], tot_in.at[me], tt_send, tt_recv,
            device_id={"sp": to}, device_id_type=MESH,
        ).start()
        return carry

    lax.fori_loop(1, N_SP, send_state, 0)
    for load in loads[6:]:
        load.start()
    w_pairs = ((wg_hbm, wg_s), (wu_hbm, wu_s), (wd_hbm, wd_s))
    own_w = [
        pltpu.make_async_copy(s.at[0], t.at[0], w_own_sem.at[i]) for i, (s, t) in enumerate(w_pairs)
    ]
    far_w = [
        pltpu.make_async_remote_copy(
            s.at[0], t.at[1], w_send.at[i], w_recv.at[i],
            device_id={"tp": other}, device_id_type=MESH,
        )
        for i, (s, t) in enumerate(w_pairs)
    ]
    for copy in own_w + far_w:
        copy.start()
    st_in[me] = st_out[me]
    tot_in[me] = tot_out[(me & 31) >> 2]

    loads[4].wait()
    even = iota((ROWS, 128), 1) < 64
    ahead_mask = iota((ROWS, 256), 0) >= (iota((ROWS, 256), 1) & (ROWS - 1))
    zero = jnp.zeros((ROWS, 128), BF16)

    def both(x):
        return jnp.concatenate([jnp.where(even, x, zero), jnp.where(even, zero, x)], axis=0)

    def local_pair(p, carry):
        total = from_s[:, lanes(p)]
        query = q_s[:, lanes(p)].astype(F32) * 0.125
        key = k_s[:, lanes(p)].astype(F32)
        value = v_s[:, lanes(p)]
        last = total[TOK - 1 :, :]
        qcat_s[:, pl.ds(pl.multiple_of(p * 256, 256), 128)] = (query * jnp.exp(total)).astype(BF16)
        qcat_s[:, pl.ds(pl.multiple_of(p * 256 + 128, 128), 128)] = (
            query * jnp.exp(last - total)
        ).astype(BF16)
        mid_total = total[ROWS - 1 : ROWS, :]
        across = jnp.exp(-jnp.abs(total - mid_total))
        query_across = (query * across).astype(BF16)
        key_across = (key * across).astype(BF16)
        for b in range(2):
            rows = slice(ROWS * b, ROWS * b + ROWS)
            far = slice(ROWS * (1 - b), ROWS * (1 - b) + ROWS)
            center = total[rows] - total[ROWS * b + 63 : ROWS * b + 64, :]
            grow = jnp.exp(center)
            fade = jnp.exp(-center)
            ahead = dot_nt((query[rows] * grow).astype(BF16), both((key[rows] * fade).astype(BF16)))
            behind = dot_nt(
                (query[rows] * fade).astype(BF16), both((key[rows] * grow).astype(BF16))
            )
            scores = jnp.where(ahead_mask, ahead, behind).astype(BF16)
            result = dot(scores, both(value[rows]))
            state = dot_tn(value[far], key_across[far])
            state = jnp.where((iota((128, 128), 0) < 64) == even, state, 0.0).astype(BF16)
            result = result + dot_nt(query_across[rows], state)
            local_s[rows, lanes(p)] = result
        return carry

    lax.fori_loop(0, PAIRS, local_pair, 0)

    lane = iota((ROWS, N_SP * CAP), 1)
    expert = shifted(me, offset_of(lane >> 3), 1)
    first = routes_ref[:, 0:1] == expert
    second = routes_ref[:, 1:2] == expert
    named = jnp.where(first | second, 1.0, 0.0)
    strict = jnp.where(iota((ROWS, ROWS), 0) > iota((ROWS, ROWS), 1), 1.0, 0.0).astype(BF16)
    rank = dot(strict, named.astype(BF16))
    chosen = (named > 0.5) & (rank == (lane & (CAP - 1)).astype(F32))
    pick = jnp.where(chosen, 1.0, 0.0).astype(BF16)
    weight = jnp.where(chosen, jnp.where(first, rw_ref[:, 0:1], rw_ref[:, 1:2]), 0.0)
    weight_hi = weight.astype(BF16)
    weight_lo = (weight - weight_hi.astype(F32)).astype(BF16)
    for c in range(CHUNKS):
        part = slice(ROWS * c, ROWS * c + ROWS)
        pick_s[c] = pick[:, part]
        comb_s[c, :ROWS] = weight_hi[:, part]
        comb_s[c, ROWS:] = weight_lo[:, part]

    def drain(buffer, count, send, recv):
        done = pltpu.make_async_remote_copy(
            buffer.at[pl.ds(0, count)], buffer.at[pl.ds(0, count)], send, recv,
            device_id={"tp": other}, device_id_type=MESH,
        )
        return done

    drain(st_in, N_SP - 1, st_send, st_recv).wait_recv()
    drain(tot_in, N_SP - 1, tt_send, tt_recv).wait_recv()
    backward = me >= 32

    def scan_step(i, state):
        at = jnp.where(backward, N_SP - 1 - i, i)
        sc_out[at] = state.astype(BF16)
        return state * tot_in[at] + st_in[at].astype(F32)

    lax.fori_loop(0, N_SP, scan_step, jnp.zeros((16, 128), F32), unroll=4)

    def send_scan(i, carry):
        to = shifted(me, offset_of(i), 1)
        pltpu.make_async_remote_copy(
            sc_out.at[to], inc_s.at[me], sc_send, sc_recv,
            device_id={"sp": to}, device_id_type=MESH,
        ).start()
        return carry

    lax.fori_loop(1, N_SP, send_scan, 0)
    inc_s[me] = sc_out[me]
    loads[5].wait()
    loads[6].wait()
    loads[7].wait()
    drain(inc_s, N_SP - 1, sc_send, sc_recv).wait_recv()

    block_mean = jnp.where((iota((128, 128), 0) < 64) == even, 1.0 / 64.0, 0.0).astype(BF16)
    gain = jnp.concatenate([hgain_ref[...], hgain_ref[...]], axis=1)
    hzero = jnp.zeros((64, 128), BF16)

    def mix_pair(p, carry):
        left = jnp.concatenate([inc_s[4 * p + part] for part in range(4)], axis=0)
        right = jnp.concatenate([inc_s[32 + 4 * p + part] for part in range(4)], axis=0)
        state = jnp.concatenate(
            [
                jnp.concatenate([jnp.where(half64, left, hzero), jnp.where(half64, right, hzero)], axis=1),
                jnp.concatenate([jnp.where(half64, hzero, left), jnp.where(half64, hzero, right)], axis=1),
            ],
            axis=0,
        )
        mixed = local_s[:, lanes(p)] + dot_nt(qcat_s[:, lanes(p, 256)], state)
        square = mixed * mixed
        square_hi = square.astype(BF16)
        square_lo = (square - square_hi.astype(F32)).astype(BF16)
        mean = dot(square_hi, block_mean) + dot(square_lo, block_mean)
        gate = silu(g_s[:, lanes(p)].astype(F32))
        gated_s[:, lanes(p)] = (mixed * lax.rsqrt(mean + EPS) * gain * gate).astype(BF16)
        return carry

    lax.fori_loop(0, PAIRS, mix_pair, 0)

    def send_partial(n):
        return pltpu.make_async_remote_copy(
            pr_out.at[n], pr_in.at[n], pr_send.at[n], pr_recv.at[n],
            device_id={"tp": other}, device_id_type=MESH,
        )

    def project(n, carry):
        part = dot(gated_s[...], wo_s[:, lanes(n, 512)]).astype(BF16)
        mine, theirs = part[:ROWS], part[ROWS:]
        own_s[:, lanes(n, 512)] = jnp.where(core == 0, mine, theirs)
        pr_out[n] = jnp.where(core == 0, theirs, mine)
        send_partial(n).start()
        return carry

    lax.fori_loop(0, 4, project, 0)

    def residual_sum(n, total):
        send_partial(n).wait_recv()
        r = res_s[:, lanes(n, 512)].astype(F32) + (
            own_s[:, lanes(n, 512)].astype(F32) + pr_in[n].astype(F32)
        )
        acc_s[:, lanes(n, 512)] = r
        return total + jnp.sum(r, axis=1, keepdims=True)

    def norm_to(target, gain_ref, total):
        mean = total * (1.0 / WIDE)

        def spread(n, s):
            d = acc_s[:, lanes(n, 512)] - mean
            return s + jnp.sum(d * d, axis=1, keepdims=True)

        var = lax.fori_loop(0, 4, spread, jnp.zeros((ROWS, 1), F32)) * (1.0 / WIDE)
        scale = lax.rsqrt(var + EPS)

        def write(n, carry):
            d = acc_s[:, lanes(n, 512)] - mean
            target[:, lanes(n, 512)] = (d * scale * gain_ref[:, lanes(n, 512)]).astype(BF16)
            return carry

        lax.fori_loop(0, 4, write, 0)

    norm_to(
        normed_s, mgain_ref, lax.fori_loop(0, 4, residual_sum, jnp.zeros((ROWS, 1), F32))
    )

    def dispatch(c, carry):
        for n in range(4):
            rows = dot_tn(pick_s[c], normed_s[:, 512 * n : 512 * n + 512])
            dsp_out[pl.ds(c * PER, PER), :, 512 * n : 512 * n + 512] = rows.reshape(
                PER, CAP, 512
            ).astype(BF16)

        def send(j, carry):
            i = c * PER + j

            @pl.when(i > 0)
            def _():
                pltpu.make_async_remote_copy(
                    dsp_out.at[i], dsp_in.at[i], d_send, d_recv.at[c],
                    device_id={"sp": shifted(me, offset_of(i), 1)}, device_id_type=MESH,
                ).start()

            return carry

        lax.fori_loop(0, PER, send, 0)
        return carry

    lax.fori_loop(0, CHUNKS, dispatch, 0)
    dsp_in[0] = dsp_out[0]

    for load in loads[8:]:
        load.wait()

    def shared_inner(n, carry):
        gate = dot(normed_s[...], cg_s[:, lanes(n, 256)])
        up = dot(normed_s[...], cu_s[:, lanes(n, 256)])
        inner_s[:, lanes(n, 256)] = (silu(gate) * up).astype(BF16)
        return carry

    lax.fori_loop(0, 2, shared_inner, 0)

    def shared_down(n, carry):
        down = dot(inner_s[:, 0:512], cd_s[:, lanes(n, 512)])
        acc_s[:, lanes(n, 512)] = normed_s[:, lanes(n, 512)].astype(F32) + down
        return carry

    lax.fori_loop(0, 4, shared_down, 0)

    for copy in own_w:
        copy.wait()
    for copy in far_w:
        copy.wait()

    def expert_chunk(c, first):
        xb_s[...] = dsp_in[pl.ds(c * PER, PER)].astype(F32).reshape(ROWS, WIDE).astype(BF16)

        def inner(t, carry):
            h, n = t >> 1, t & 1
            gate = dot(xb_s[...], wg_s[h, :, lanes(n, 256)])
            up = dot(xb_s[...], wu_s[h, :, lanes(n, 256)])
            inner_s[:, lanes(t, 256)] = (silu(gate) * up).astype(BF16)
            return carry

        lax.fori_loop(0, 4, inner, 0)

        def down(n, carry):
            result = dot(inner_s[:, 0:512], wd_s[0, :, lanes(n, 512)])
            result = result + dot(inner_s[:, 512:1024], wd_s[1, :, lanes(n, 512)])
            e_out[pl.ds(c * PER, PER), :, lanes(n, 512)] = result.reshape(PER, CAP, 512).astype(BF16)
            return carry

        lax.fori_loop(0, 4, down, 0)

        def send(j, carry):
            i = c * PER + j

            @pl.when(i > 0)
            def _():
                pltpu.make_async_remote_copy(
                    e_out.at[i], ret_s.at[i], r_send, r_recv.at[c],
                    device_id={"sp": shifted(me, offset_of(i), -1)}, device_id_type=MESH,
                ).start()

            return carry

        lax.fori_loop(0, PER, send, 0)

    def arrived(buffer, c, recv):
        def wait(count):
            pltpu.make_async_remote_copy(
                buffer.at[pl.ds(0, count)], buffer.at[pl.ds(0, count)], d_send, recv.at[c],
                device_id={"tp": other}, device_id_type=MESH,
            ).wait_recv()

        @pl.when(c == 0)
        def _():
            wait(PER - 1)

        @pl.when(c > 0)
        def _():
            wait(PER)

    def experts(c, carry):
        arrived(dsp_in, c, d_recv)
        expert_chunk(c, 0)
        return carry

    lax.fori_loop(0, CHUNKS, experts, 0)
    ret_s[0] = e_out[0]

    def combine(c, carry):
        arrived(ret_s, c, r_recv)

        def part(n, carry):
            rows = ret_s[pl.ds(c * PER, PER), :, lanes(n, 512)]
            rows = rows.astype(F32).reshape(ROWS, 512).astype(BF16)
            both_parts = dot(comb_s[c], rows)
            acc_s[:, lanes(n, 512)] += both_parts[:ROWS] + both_parts[ROWS:]
            return carry

        lax.fori_loop(0, 4, part, 0)
        return carry

    lax.fori_loop(0, CHUNKS, combine, 0)

    def total_of(n, total):
        return total + jnp.sum(acc_s[:, lanes(n, 512)], axis=1, keepdims=True)

    norm_to(out_ref, fgain_ref, lax.fori_loop(0, 4, total_of, jnp.zeros((ROWS, 1), F32)))

    drain(st_in, N_SP - 1, st_send, st_recv).wait_send()
    drain(tot_in, N_SP - 1, tt_send, tt_recv).wait_send()
    drain(inc_s, N_SP - 1, sc_send, sc_recv).wait_send()
    drain(dsp_in, N_SP - 1, d_send, d_recv.at[0]).wait_send()
    drain(ret_s, N_SP - 1, r_send, r_recv.at[0]).wait_send()

    def partial_left(n, carry):
        send_partial(n).wait_send()
        return carry

    lax.fori_loop(0, 4, partial_left, 0)


def per_device(
    q, k, v, g, a, x, res, hgain, wo, mgain, routes, rw, wg, wu, wd, cg, cu, cd, fgain
):
    anywhere = pl.BlockSpec(memory_space=pl.ANY)
    vmem = pl.BlockSpec(memory_space=pltpu.VMEM)
    specs = [anywhere] * 7 + [vmem, anywhere, vmem, vmem, vmem] + [anywhere] * 6 + [vmem]
    dma = pltpu.SemaphoreType.DMA
    scratch = [
        pltpu.VMEM((TOK, 1024), BF16),
        pltpu.VMEM((TOK, 1024), BF16),
        pltpu.VMEM((TOK, 1024), BF16),
        pltpu.VMEM((TOK, 1024), BF16),
        pltpu.VMEM((TOK, 1024), BF16),
        pltpu.VMEM((TOK, 16), F32),
        pltpu.VMEM((ROWS, WIDE), BF16),
        pltpu.VMEM((1024, WIDE), BF16),
        pltpu.VMEM((WIDE, 512), BF16),
        pltpu.VMEM((WIDE, 512), BF16),
        pltpu.VMEM((512, WIDE), BF16),
        pltpu.VMEM((2, WIDE, 512), BF16),
        pltpu.VMEM((2, WIDE, 512), BF16),
        pltpu.VMEM((2, 512, WIDE), BF16),
        pltpu.VMEM((TOK, 1024), F32),
        pltpu.VMEM((TOK, 1024), F32),
        pltpu.VMEM((TOK, WIDE), BF16),
        pltpu.VMEM((N_SP, 16, 128), BF16),
        pltpu.VMEM((N_SP, 16, 128), BF16),
        pltpu.VMEM((PAIRS, 1, 128), F32),
        pltpu.VMEM((N_SP, 1, 128), F32),
        pltpu.VMEM((N_SP, 16, 128), BF16),
        pltpu.VMEM((N_SP, 16, 128), BF16),
        pltpu.VMEM((TOK, 1024), BF16),
        pltpu.VMEM((ROWS, WIDE), BF16),
        pltpu.VMEM((4, ROWS, 512), BF16),
        pltpu.VMEM((4, ROWS, 512), BF16),
        pltpu.VMEM((ROWS, WIDE), BF16),
        pltpu.VMEM((CHUNKS, ROWS, ROWS), BF16),
        pltpu.VMEM((CHUNKS, 2 * ROWS, ROWS), BF16),
        pltpu.VMEM((N_SP, CAP, WIDE), BF16),
        pltpu.VMEM((N_SP, CAP, WIDE), BF16),
        pltpu.VMEM((ROWS, WIDE), BF16),
        pltpu.VMEM((ROWS, 1024), BF16),
        pltpu.VMEM((N_SP, CAP, WIDE), BF16),
        pltpu.VMEM((N_SP, CAP, WIDE), BF16),
        pltpu.VMEM((ROWS, WIDE), F32),
        dma((11,)), dma((3,)), dma((3,)), dma((3,)),
        dma, dma, dma, dma, dma, dma,
        dma((4,)), dma((4,)),
        dma, dma((CHUNKS,)), dma, dma((CHUNKS,)),
    ]
    return pl.pallas_call(
        layer_kernel,
        name="layer",
        out_shape=jax.ShapeDtypeStruct((ROWS, WIDE), BF16),
        in_specs=specs,
        out_specs=vmem,
        scratch_shapes=scratch,
        compiler_params=pltpu.CompilerParams(
            collective_id=0, has_side_effects=True, vmem_limit_bytes=60 * 1024 * 1024
        ),
    )(
        q, k, v, g, a, x, res, hgain.reshape(1, -1), wo, mgain.reshape(1, -1), routes, rw,
        wg, wu, wd, cg, cu, cd, fgain.reshape(1, -1),
    )


def solution(mesh):
    return jax.shard_map(
        per_device,
        mesh=mesh,
        in_specs=(
            P("sp", "tp"),
            P("sp", "tp"),
            P("sp", "tp"),
            P("sp", "tp"),
            P("sp", "tp"),
            P("sp", "tp"),
            P(SP_TP, None),
            P(),
            P("tp", None),
            P(),
            P(SP_TP, None),
            P(SP_TP, None),
            P("sp", None, "tp"),
            P("sp", None, "tp"),
            P("sp", "tp", None),
            P(),
            P(),
            P(),
            P(),
        ),
        out_specs=P(SP_TP, None),
        check_vma=False,
    )
```

time: 416 us -> 96.2 us (0.23)
  blocking collectives: 159 us -> 0 us
  waiting for transfers between devices: 95.8 us -> 0 us
  Pallas kernels: 0 us -> 89.7 us
  matrix products: 59 us -> 0 us
  other arithmetic: 38.8 us -> 0 us
  local copies, waits for them, and re-layouts: 37.7 us -> 6.16 us
  between operations: 13.6 us -> 0.01 us
  starting transfers between devices: 10.5 us -> 0 us
    all_gather x11 -> x0, blocking collectives: 119 us -> none  [entering(): lax.all_gather(part.astype(kind), axis)]
    pallas_call x0 -> x1, Pallas kernels: none -> 89.7 us  [per_device(): pl.pallas_call(layer_kernel, name='layer', out_shape=jax.ShapeDtypeStruct...]
    dot_general x14 -> x0, matrix products: 59 us -> none  [the longest x1 10 us: expert_half(): jnp.dot(inner, down_half, preferred_element_type=jnp.float32)]
    reduce_scatter x2 -> x0, waiting for transfers between devices: 54.4 us -> none  [the longest x1 38.2 us: per_device(): lax.psum_scatter(jnp.dot(gated, output_projection_weight, preferred_eleme...]
    all_to_all x1 -> x0, blocking collectives: 39.3 us -> none  [per_device(): lax.all_to_all(outbound, SP, split_axis=0, concat_axis=0, tiled=True)]
    all_to_all x1 -> x0, waiting for transfers between devices: 26.6 us -> none  [per_device(): lax.all_to_all(summed, SP, split_axis=0, concat_axis=0, tiled=True)]
    all_gather x1 -> x0, waiting for transfers between devices: 14.8 us -> none  [per_device(): lax.all_gather(lax.all_to_all(outbound, SP, split_axis=0, concat_axis=0,...]
    add x8 -> x0, other arithmetic: 10.7 us -> none  [carry_step(): return (jnp.exp(total)[..., None] * carried + summed, carried)]
  transfers between devices with their start and end apart: 4 -> 0, of which waited for: 4 -> 0; matrix products, arithmetic and copies ran while one was open for 1% -> 0% of each run, Pallas kernels for 0% -> 0%
where the time goes in v1:
time: 96.2 us; the launch traced here: 95.9 us
  Pallas kernels  89.7 us (93%)
  local copies, waits for them, and re-layouts  6.16 us (6%)
    pallas_call x1, Pallas kernels, per_device(): pl.pallas_call(layer_kernel, name='layer', out_shape=jax.ShapeDtypeStruct...  89.7 us
    unnamed x4, local copies, waits for them, and re-layouts  6.16 us

profile of v1, /device:TPU:1, one launch (start us, length us, event | category | flops | bytes accessed | tf_op | source)
XLA Modules:
  0.0 95.9 jit_solution(3620107818206873283)
XLA Ops:
  0.0 1.4 %copy.21.routes_ref = s32[128,2]{1,0:T(8,128)} copy(s32[128,2]{0,1:T(2,128)} %param.29) | data formatting | bytes 2048 | tf_op args[10]
  1.4 1.4 %copy.22.rw_ref = f32[128,2]{1,0:T(8,128)} copy(f32[128,2]{0,1:T(2,128)} %param.30) | data formatting | bytes 2048 | tf_op args[11]
  2.8 1.5 %copy.20.x_hbm = f32[256,16]{1,0:T(8,128)} copy(f32[256,16]{0,1:T(8,128)} %param.24) | data formatting | bytes 32768 | tf_op args[5]
  4.3 89.7 %layer.1 = bf16[128,2048]{1,0:T(8,128)(2,1)} custom-call(bf16[256,1024]{1,0:T(8,128)(2,1)} %q_hbm.1, bf16[256,1024]{1,0:T(8,128)(2,1)} %k_hbm.1, bf16[256,1024]{1,0:T(8,128)(2,1)} %v_hbm.1, bf16[256,1024]{1,0:T(8,128)(2,1)} %g_hbm.1, bf16[256,1024]{1,0:T(8,128)(2,1)} %a_hbm.1, f32[256,16]{1,0:T(8,128)} %copy.20.x_hbm, bf16[128,2048]{1,0:T(8,128)(2,1)} %res_hbm.1, ...), custom_call_target="tpu_custom_call" | custom-call | tf_op jit(solution)/shard_map/layer/pallas_call | solution.py:522
  94.0 1.9 %copy.24 = bf16[128,2048]{1,0:T(8,128)(2,1)} copy(bf16[128,2048]{1,0:T(8,128)(2,1)} %layer.1) | data formatting | bytes 1048576

commit v2 on v1

--- a/solution.py
+++ b/solution.py
@@ -19,7 +19,14 @@
 CHUNKS = 4
 PER = N_SP // CHUNKS
 CAP = 8
-MIX = 27
+
+
+def hops(s):
+    return sum(min(d, 4 - d) for d in (s >> 4, (s >> 2) & 3, s & 3))
+
+
+FAR_FIRST = sorted(range(1, N_SP), key=lambda s: -hops(s))
+SLOTS = [27 * i % N_SP for i in range(N_SP)]
 
 
 def dot(a, b):
@@ -34,15 +41,9 @@
     return lax.dot_general(a, b, (((0,), (0,)), ((), ())), preferred_element_type=F32)
 
 
-def split3(x):
+def split2(x):
     hi = x.astype(BF16)
-    rest = x - hi.astype(F32)
-    mid = rest.astype(BF16)
-    return hi, mid, (rest - mid.astype(F32)).astype(BF16)
-
-
-def offset_of(i):
-    return (i * MIX) & (N_SP - 1)
+    return hi, (x - hi.astype(F32)).astype(BF16)
 
 
 def shifted(me, s, sign):
@@ -57,8 +58,7 @@
 
 
 def log_sigmoid(x):
-    t = jnp.exp(-jnp.abs(x))
-    return jnp.minimum(x, 0.0) - jnp.log1p(t)
+    return jnp.minimum(x, 0.0) - jnp.log(1.0 + jnp.exp(-jnp.abs(x)))
 
 
 def lanes(p, width=128):
@@ -75,7 +75,7 @@
     out_ref,
     q_s, k_s, v_s, g_s, a_s, x_s, res_s, wo_s, cg_s, cu_s, cd_s, wg_s, wu_s, wd_s,
     from_s, local_s, qcat_s, st_out, st_in, tot_out, tot_in, sc_out, inc_s,
-    gated_s, own_s, pr_out, pr_in, normed_s, pick_s, comb_s,
+    gate_s, gated_s, own_s, pr_out, pr_in, normed_s, pick_s, comb_s,
     dsp_out, dsp_in, xb_s, inner_s, e_out, ret_s, acc_s,
     ld_sem, w_own_sem, w_send, w_recv, st_send, st_recv, tt_send, tt_recv, sc_send, sc_recv,
     pr_send, pr_recv, d_send, d_recv, r_send, r_recv,
@@ -94,13 +94,10 @@
 
     barrier = pltpu.get_barrier_semaphore()
 
-    def greet(s, carry):
+    for s in FAR_FIRST:
         pl.semaphore_signal(
             barrier, inc=1, device_id={"sp": shifted(me, s, 1)}, device_id_type=MESH
         )
-        return carry
-
-    lax.fori_loop(1, N_SP, greet, 0)
     pl.semaphore_signal(barrier, inc=1, device_id={"tp": other}, device_id_type=MESH)
 
     low = iota((TOK, TOK), 0) >= iota((TOK, TOK), 1)
@@ -108,37 +105,51 @@
     half64 = iota((64, 128), 1) < 64
     for load in loads[:4]:
         load.wait()
+    w_pairs = ((wg_hbm, wg_s), (wu_hbm, wu_s), (wd_hbm, wd_s))
+    own_w = [
+        pltpu.make_async_copy(s.at[0], t.at[0], w_own_sem.at[i]) for i, (s, t) in enumerate(w_pairs)
+    ]
+    far_w = [
+        pltpu.make_async_remote_copy(
+            s.at[0], t.at[1], w_send.at[i], w_recv.at[i],
+            device_id={"tp": other}, device_id_type=MESH,
+        )
+        for i, (s, t) in enumerate(w_pairs)
+    ]
+    for load in loads[6:] + own_w:
+        load.start()
+
+    added_hi = x_s[...].astype(BF16)
+    rest = x_s[...] - added_hi.astype(F32)
+    added = jnp.concatenate([added_hi.astype(F32)] + [r.astype(F32) for r in split2(rest)], axis=0)
+    added = added.T.astype(BF16)
 
     def own_state(p, carry):
+        spread = jnp.where((iota((48, 128), 0) & 15) == 2 * p + (iota((48, 128), 1) >> 6), 1.0, 0.0)
         decay = log_sigmoid(a_s[:, lanes(p)].astype(F32)) * (1.0 / 16.0)
-        spread = jnp.where(iota((16, 128), 0) == 2 * p + (iota((16, 128), 1) >> 6), 1.0, 0.0)
-        spread = spread.astype(BF16)
-        for part in split3(x_s[...]):
-            decay = decay + dot(part, spread)
-        hi, mid, lo = split3(decay)
-        total = dot(low_bf, hi) + dot(low_bf, mid) + dot(low_bf, lo)
+        decay = decay + dot(added, spread.astype(BF16))
+        summed = dot(low_bf, jnp.concatenate(split2(decay), axis=1))
+        total = summed[:, :128] + summed[:, 128:]
         from_s[:, lanes(p)] = total
         last = total[TOK - 1 :, :]
         tot_out[p] = jnp.exp(last)
         key = k_s[:, lanes(p)].astype(F32)
         up = (key * jnp.exp(total)).astype(BF16)
         end = (key * jnp.exp(last - total)).astype(BF16)
-        value = v_s[:, lanes(p)]
-        left = dot_tn(value, end)
-        right = dot_tn(value, up)
-        left = jnp.where(half64, left[:64], left[64:]).astype(BF16)
-        right = jnp.where(half64, right[:64], right[64:]).astype(BF16)
+        state = dot_tn(v_s[:, lanes(p)], jnp.concatenate([end, up], axis=1))
+        left = jnp.where(half64, state[:64, :128], state[64:, :128]).astype(BF16)
+        right = jnp.where(half64, state[:64, 128:], state[64:, 128:]).astype(BF16)
         for part in range(4):
             st_out[4 * p + part] = left[16 * part : 16 * part + 16]
             st_out[32 + 4 * p + part] = right[16 * part : 16 * part + 16]
         return carry
 
-    lax.fori_loop(0, PAIRS, own_state, 0)
+    lax.fori_loop(0, PAIRS, own_state, 0, unroll=2)
 
     pl.semaphore_wait(barrier, N_SP)
 
-    def send_state(i, carry):
-        to = shifted(me, offset_of(i), 1)
+    for s in FAR_FIRST:
+        to = shifted(me, s, 1)
         pltpu.make_async_remote_copy(
             st_out.at[to], st_in.at[me], st_send, st_recv,
             device_id={"sp": to}, device_id_type=MESH,
@@ -147,24 +158,6 @@
             tot_out.at[(to & 31) >> 2], tot_in.at[me], tt_send, tt_recv,
             device_id={"sp": to}, device_id_type=MESH,
         ).start()
-        return carry
-
-    lax.fori_loop(1, N_SP, send_state, 0)
-    for load in loads[6:]:
-        load.start()
-    w_pairs = ((wg_hbm, wg_s), (wu_hbm, wu_s), (wd_hbm, wd_s))
-    own_w = [
-        pltpu.make_async_copy(s.at[0], t.at[0], w_own_sem.at[i]) for i, (s, t) in enumerate(w_pairs)
-    ]
-    far_w = [
-        pltpu.make_async_remote_copy(
-            s.at[0], t.at[1], w_send.at[i], w_recv.at[i],
-            device_id={"tp": other}, device_id_type=MESH,
-        )
-        for i, (s, t) in enumerate(w_pairs)
-    ]
-    for copy in own_w + far_w:
-        copy.start()
     st_in[me] = st_out[me]
     tot_in[me] = tot_out[(me & 31) >> 2]
 
@@ -208,25 +201,29 @@
             local_s[rows, lanes(p)] = result
         return carry
 
-    lax.fori_loop(0, PAIRS, local_pair, 0)
-
-    lane = iota((ROWS, N_SP * CAP), 1)
-    expert = shifted(me, offset_of(lane >> 3), 1)
-    first = routes_ref[:, 0:1] == expert
-    second = routes_ref[:, 1:2] == expert
-    named = jnp.where(first | second, 1.0, 0.0)
-    strict = jnp.where(iota((ROWS, ROWS), 0) > iota((ROWS, ROWS), 1), 1.0, 0.0).astype(BF16)
-    rank = dot(strict, named.astype(BF16))
-    chosen = (named > 0.5) & (rank == (lane & (CAP - 1)).astype(F32))
-    pick = jnp.where(chosen, 1.0, 0.0).astype(BF16)
-    weight = jnp.where(chosen, jnp.where(first, rw_ref[:, 0:1], rw_ref[:, 1:2]), 0.0)
-    weight_hi = weight.astype(BF16)
-    weight_lo = (weight - weight_hi.astype(F32)).astype(BF16)
+    lax.fori_loop(0, PAIRS // 2, local_pair, 0)
+
+    strict = jnp.where(iota((ROWS, ROWS), 0) < iota((ROWS, ROWS), 1), 1.0, 0.0).astype(BF16)
+    slot = iota((ROWS, ROWS), 0)
+
     for c in range(CHUNKS):
-        part = slice(ROWS * c, ROWS * c + ROWS)
-        pick_s[c] = pick[:, part]
-        comb_s[c, :ROWS] = weight_hi[:, part]
-        comb_s[c, ROWS:] = weight_lo[:, part]
+        expert = jnp.concatenate(
+            [
+                jnp.full((CAP, ROWS), shifted(me, s, 1), jnp.int32)
+                for s in SLOTS[PER * c : PER * c + PER]
+            ],
+            axis=0,
+        )
+        first = routes_ref[0:1, :] == expert
+        second = routes_ref[1:2, :] == expert
+        named = jnp.where(first | second, 1.0, 0.0)
+        rank = dot(named.astype(BF16), strict)
+        chosen = (named > 0.5) & (rank == (slot & (CAP - 1)).astype(F32))
+        pick_s[c] = jnp.where(chosen, 1.0, 0.0).astype(BF16)
+        weight = jnp.where(chosen, jnp.where(first, rw_ref[0:1, :], rw_ref[1:2, :]), 0.0).T
+        weight_hi = weight.astype(BF16)
+        comb_s[c, :ROWS] = weight_hi
+        comb_s[c, ROWS:] = (weight - weight_hi.astype(F32)).astype(BF16)
 
     def drain(buffer, count, send, recv):
         done = pltpu.make_async_remote_copy(
@@ -244,25 +241,31 @@
         sc_out[at] = state.astype(BF16)
         return state * tot_in[at] + st_in[at].astype(F32)
 
-    lax.fori_loop(0, N_SP, scan_step, jnp.zeros((16, 128), F32), unroll=4)
-
-    def send_scan(i, carry):
-        to = shifted(me, offset_of(i), 1)
+    lax.fori_loop(0, N_SP, scan_step, jnp.zeros((16, 128), F32), unroll=16)
+
+    for s in FAR_FIRST:
+        to = shifted(me, s, 1)
         pltpu.make_async_remote_copy(
             sc_out.at[to], inc_s.at[me], sc_send, sc_recv,
             device_id={"sp": to}, device_id_type=MESH,
         ).start()
-        return carry
-
-    lax.fori_loop(1, N_SP, send_scan, 0)
     inc_s[me] = sc_out[me]
+    lax.fori_loop(PAIRS // 2, PAIRS, local_pair, 0)
     loads[5].wait()
+    gain = jnp.concatenate([hgain_ref[...], hgain_ref[...]], axis=1)
+
+    def gates(p, carry):
+        gate_s[:, lanes(p)] = silu(g_s[:, lanes(p)].astype(F32)) * gain
+        return carry
+
+    lax.fori_loop(0, PAIRS, gates, 0)
     loads[6].wait()
     loads[7].wait()
     drain(inc_s, N_SP - 1, sc_send, sc_recv).wait_recv()
 
-    block_mean = jnp.where((iota((128, 128), 0) < 64) == even, 1.0 / 64.0, 0.0).astype(BF16)
-    gain = jnp.concatenate([hgain_ref[...], hgain_ref[...]], axis=1)
+    block_mean = jnp.where(
+        ((iota((TOK, 128), 0) >> 6) & 1) == (iota((TOK, 128), 1) >> 6), 1.0 / 64.0, 0.0
+    ).astype(BF16)
     hzero = jnp.zeros((64, 128), BF16)
 
     def mix_pair(p, carry):
@@ -276,15 +279,11 @@
             axis=0,
         )
         mixed = local_s[:, lanes(p)] + dot_nt(qcat_s[:, lanes(p, 256)], state)
-        square = mixed * mixed
-        square_hi = square.astype(BF16)
-        square_lo = (square - square_hi.astype(F32)).astype(BF16)
-        mean = dot(square_hi, block_mean) + dot(square_lo, block_mean)
-        gate = silu(g_s[:, lanes(p)].astype(F32))
-        gated_s[:, lanes(p)] = (mixed * lax.rsqrt(mean + EPS) * gain * gate).astype(BF16)
-        return carry
-
-    lax.fori_loop(0, PAIRS, mix_pair, 0)
+        mean = dot(jnp.concatenate(split2(mixed * mixed), axis=1), block_mean)
+        gated_s[:, lanes(p)] = (mixed * lax.rsqrt(mean + EPS) * gate_s[:, lanes(p)]).astype(BF16)
+        return carry
+
+    lax.fori_loop(0, PAIRS, mix_pair, 0, unroll=4)
 
     def send_partial(n):
         return pltpu.make_async_remote_copy(
@@ -300,7 +299,7 @@
         send_partial(n).start()
         return carry
 
-    lax.fori_loop(0, 4, project, 0)
+    lax.fori_loop(0, 4, project, 0, unroll=True)
 
     def residual_sum(n, total):
         send_partial(n).wait_recv()
@@ -317,7 +316,7 @@
             d = acc_s[:, lanes(n, 512)] - mean
             return s + jnp.sum(d * d, axis=1, keepdims=True)
 
-        var = lax.fori_loop(0, 4, spread, jnp.zeros((ROWS, 1), F32)) * (1.0 / WIDE)
+        var = lax.fori_loop(0, 4, spread, jnp.zeros((ROWS, 1), F32), unroll=True) * (1.0 / WIDE)
         scale = lax.rsqrt(var + EPS)
 
         def write(n, carry):
@@ -325,35 +324,27 @@
             target[:, lanes(n, 512)] = (d * scale * gain_ref[:, lanes(n, 512)]).astype(BF16)
             return carry
 
-        lax.fori_loop(0, 4, write, 0)
+        lax.fori_loop(0, 4, write, 0, unroll=True)
 
     norm_to(
-        normed_s, mgain_ref, lax.fori_loop(0, 4, residual_sum, jnp.zeros((ROWS, 1), F32))
+        normed_s, mgain_ref, lax.fori_loop(0, 4, residual_sum, jnp.zeros((ROWS, 1), F32), unroll=True)
     )
 
-    def dispatch(c, carry):
-        for n in range(4):
-            rows = dot_tn(pick_s[c], normed_s[:, 512 * n : 512 * n + 512])
-            dsp_out[pl.ds(c * PER, PER), :, 512 * n : 512 * n + 512] = rows.reshape(
-                PER, CAP, 512
-            ).astype(BF16)
-
-        def send(j, carry):
-            i = c * PER + j
-
-            @pl.when(i > 0)
-            def _():
-                pltpu.make_async_remote_copy(
-                    dsp_out.at[i], dsp_in.at[i], d_send, d_recv.at[c],
-                    device_id={"sp": shifted(me, offset_of(i), 1)}, device_id_type=MESH,
-                ).start()
-
+    for c in range(CHUNKS):
+
+        def fill(n, carry):
+            rows = dot(pick_s[c], normed_s[:, lanes(n, 512)])
+            dsp_out[c * PER : c * PER + PER, :, lanes(n, 512)] = rows.reshape(PER, CAP, 512).astype(BF16)
             return carry
 
-        lax.fori_loop(0, PER, send, 0)
-        return carry
-
-    lax.fori_loop(0, CHUNKS, dispatch, 0)
+        lax.fori_loop(0, 4, fill, 0)
+        for i in range(max(1, c * PER), c * PER + PER):
+            pltpu.make_async_remote_copy(
+                dsp_out.at[i], dsp_in.at[i], d_send, d_recv.at[c],
+                device_id={"sp": shifted(me, SLOTS[i], 1)}, device_id_type=MESH,
+            ).start()
+    for copy in far_w:
+        copy.start()
     dsp_in[0] = dsp_out[0]
 
     for load in loads[8:]:
@@ -379,8 +370,16 @@
     for copy in far_w:
         copy.wait()
 
-    def expert_chunk(c, first):
-        xb_s[...] = dsp_in[pl.ds(c * PER, PER)].astype(F32).reshape(ROWS, WIDE).astype(BF16)
+    def arrived(buffer, c, recv):
+        count = PER if c else PER - 1
+        pltpu.make_async_remote_copy(
+            buffer.at[pl.ds(0, count)], buffer.at[pl.ds(0, count)], d_send, recv.at[c],
+            device_id={"tp": other}, device_id_type=MESH,
+        ).wait_recv()
+
+    for c in range(CHUNKS):
+        arrived(dsp_in, c, d_recv)
+        xb_s[...] = dsp_in[c * PER : c * PER + PER].astype(F32).reshape(ROWS, WIDE).astype(BF16)
 
         def inner(t, carry):
             h, n = t >> 1, t & 1
@@ -394,67 +393,33 @@
         def down(n, carry):
             result = dot(inner_s[:, 0:512], wd_s[0, :, lanes(n, 512)])
             result = result + dot(inner_s[:, 512:1024], wd_s[1, :, lanes(n, 512)])
-            e_out[pl.ds(c * PER, PER), :, lanes(n, 512)] = result.reshape(PER, CAP, 512).astype(BF16)
+            e_out[c * PER : c * PER + PER, :, lanes(n, 512)] = result.reshape(PER, CAP, 512).astype(BF16)
             return carry
 
         lax.fori_loop(0, 4, down, 0)
-
-        def send(j, carry):
-            i = c * PER + j
-
-            @pl.when(i > 0)
-            def _():
-                pltpu.make_async_remote_copy(
-                    e_out.at[i], ret_s.at[i], r_send, r_recv.at[c],
-                    device_id={"sp": shifted(me, offset_of(i), -1)}, device_id_type=MESH,
-                ).start()
-
+        for i in range(max(1, c * PER), c * PER + PER):
+            pltpu.make_async_remote_copy(
+                e_out.at[i], ret_s.at[i], r_send, r_recv.at[c],
+                device_id={"sp": shifted(me, SLOTS[i], -1)}, device_id_type=MESH,
+            ).start()
+    ret_s[0] = e_out[0]
+
+    for c in range(CHUNKS):
+        arrived(ret_s, c, r_recv)
+
+        def combine(n, carry):
+            rows = ret_s[c * PER : c * PER + PER, :, lanes(n, 512)]
+            rows = rows.astype(F32).reshape(ROWS, 512).astype(BF16)
+            parts = dot(comb_s[c], rows)
+            acc_s[:, lanes(n, 512)] += parts[:ROWS] + parts[ROWS:]
             return carry
 
-        lax.fori_loop(0, PER, send, 0)
-
-    def arrived(buffer, c, recv):
-        def wait(count):
-            pltpu.make_async_remote_copy(
-                buffer.at[pl.ds(0, count)], buffer.at[pl.ds(0, count)], d_send, recv.at[c],
-                device_id={"tp": other}, device_id_type=MESH,
-            ).wait_recv()
-
-        @pl.when(c == 0)
-        def _():
-            wait(PER - 1)
-
-        @pl.when(c > 0)
-        def _():
-            wait(PER)
-
-    def experts(c, carry):
-        arrived(dsp_in, c, d_recv)
-        expert_chunk(c, 0)
-        return carry
-
-    lax.fori_loop(0, CHUNKS, experts, 0)
-    ret_s[0] = e_out[0]
-
-    def combine(c, carry):
-        arrived(ret_s, c, r_recv)
-
-        def part(n, carry):
-            rows = ret_s[pl.ds(c * PER, PER), :, lanes(n, 512)]
-            rows = rows.astype(F32).reshape(ROWS, 512).astype(BF16)
-            both_parts = dot(comb_s[c], rows)
-            acc_s[:, lanes(n, 512)] += both_parts[:ROWS] + both_parts[ROWS:]
-            return carry
-
-        lax.fori_loop(0, 4, part, 0)
-        return carry
-
-    lax.fori_loop(0, CHUNKS, combine, 0)
+        lax.fori_loop(0, 4, combine, 0)
 
     def total_of(n, total):
         return total + jnp.sum(acc_s[:, lanes(n, 512)], axis=1, keepdims=True)
 
-    norm_to(out_ref, fgain_ref, lax.fori_loop(0, 4, total_of, jnp.zeros((ROWS, 1), F32)))
+    norm_to(out_ref, fgain_ref, lax.fori_loop(0, 4, total_of, jnp.zeros((ROWS, 1), F32), unroll=True))
 
     drain(st_in, N_SP - 1, st_send, st_recv).wait_send()
     drain(tot_in, N_SP - 1, tt_send, tt_recv).wait_send()
@@ -482,7 +447,7 @@
         pltpu.VMEM((TOK, 1024), BF16),
         pltpu.VMEM((TOK, 1024), BF16),
         pltpu.VMEM((TOK, 1024), BF16),
-        pltpu.VMEM((TOK, 16), F32),
+        pltpu.VMEM((16, TOK), F32),
         pltpu.VMEM((ROWS, WIDE), BF16),
         pltpu.VMEM((1024, WIDE), BF16),
         pltpu.VMEM((WIDE, 512), BF16),
@@ -500,6 +465,7 @@
         pltpu.VMEM((N_SP, 1, 128), F32),
         pltpu.VMEM((N_SP, 16, 128), BF16),
         pltpu.VMEM((N_SP, 16, 128), BF16),
+        pltpu.VMEM((TOK, 1024), F32),
         pltpu.VMEM((TOK, 1024), BF16),
         pltpu.VMEM((ROWS, WIDE), BF16),
         pltpu.VMEM((4, ROWS, 512), BF16),
@@ -530,7 +496,7 @@
             collective_id=0, has_side_effects=True, vmem_limit_bytes=60 * 1024 * 1024
         ),
     )(
-        q, k, v, g, a, x, res, hgain.reshape(1, -1), wo, mgain.reshape(1, -1), routes, rw,
+        q, k, v, g, a, x.T, res, hgain.reshape(1, -1), wo, mgain.reshape(1, -1), routes.T, rw.T,
         wg, wu, wd, cg, cu, cd, fgain.reshape(1, -1),
     )
 

time: 96.2 us -> 83.9 us (0.87)
  Pallas kernels: 89.7 us -> 81.8 us
  local copies, waits for them, and re-layouts: 6.16 us -> 1.88 us
    pallas_call x1, Pallas kernels: 89.7 us -> 81.8 us  [per_device(): pl.pallas_call(layer_kernel, name='layer', out_shape=jax.ShapeDtypeStruct...]
    unnamed x4 -> x1, local copies, waits for them, and re-layouts: 6.16 us -> 1.88 us
where the time goes in v2:
time: 83.9 us; the launch traced here: 83.7 us
  Pallas kernels  81.8 us (97%)
  local copies, waits for them, and re-layouts  1.88 us (2%)
    pallas_call x1, Pallas kernels, per_device(): pl.pallas_call(layer_kernel, name='layer', out_shape=jax.ShapeDtypeStruct...  81.8 us
    unnamed x1, local copies, waits for them, and re-layouts  1.88 us

profile of v2, /device:TPU:1, one launch (start us, length us, event | category | flops | bytes accessed | tf_op | source)
XLA Modules:
  0.0 83.7 jit_solution(16327424982874066422)
XLA Ops:
  0.0 81.8 %layer.1 = bf16[128,2048]{1,0:T(8,128)(2,1)} custom-call(bf16[256,1024]{1,0:T(8,128)(2,1)} %q_hbm.1, bf16[256,1024]{1,0:T(8,128)(2,1)} %k_hbm.1, bf16[256,1024]{1,0:T(8,128)(2,1)} %v_hbm.1, bf16[256,1024]{1,0:T(8,128)(2,1)} %g_hbm.1, bf16[256,1024]{1,0:T(8,128)(2,1)} %a_hbm.1, f32[16,256]{1,0:T(8,128)} %bitcast.6, bf16[128,2048]{1,0:T(8,128)(2,1)} %res_hbm.1, ...), custom_call_target="tpu_custom_call" | custom-call | tf_op jit(solution)/shard_map/layer/pallas_call | solution.py:488
  81.8 1.9 %copy.21 = bf16[128,2048]{1,0:T(8,128)(2,1)} copy(bf16[128,2048]{1,0:T(8,128)(2,1)} %layer.1) | data formatting | bytes 1048576

commit v3 on v2

--- a/solution.py
+++ b/solution.py
@@ -26,7 +26,7 @@
 
 
 FAR_FIRST = sorted(range(1, N_SP), key=lambda s: -hops(s))
-SLOTS = [27 * i % N_SP for i in range(N_SP)]
+SLOTS = [53 * i % N_SP for i in range(N_SP)]
 
 
 def dot(a, b):
@@ -144,7 +144,7 @@
             st_out[32 + 4 * p + part] = right[16 * part : 16 * part + 16]
         return carry
 
-    lax.fori_loop(0, PAIRS, own_state, 0, unroll=2)
+    lax.fori_loop(0, PAIRS, own_state, 0, unroll=8)
 
     pl.semaphore_wait(barrier, N_SP)
 
@@ -283,7 +283,7 @@
         gated_s[:, lanes(p)] = (mixed * lax.rsqrt(mean + EPS) * gate_s[:, lanes(p)]).astype(BF16)
         return carry
 
-    lax.fori_loop(0, PAIRS, mix_pair, 0, unroll=4)
+    lax.fori_loop(0, PAIRS, mix_pair, 0, unroll=8)
 
     def send_partial(n):
         return pltpu.make_async_remote_copy(
@@ -337,7 +337,7 @@
             dsp_out[c * PER : c * PER + PER, :, lanes(n, 512)] = rows.reshape(PER, CAP, 512).astype(BF16)
             return carry
 
-        lax.fori_loop(0, 4, fill, 0)
+        lax.fori_loop(0, 4, fill, 0, unroll=True)
         for i in range(max(1, c * PER), c * PER + PER):
             pltpu.make_async_remote_copy(
                 dsp_out.at[i], dsp_in.at[i], d_send, d_recv.at[c],
@@ -388,7 +388,7 @@
             inner_s[:, lanes(t, 256)] = (silu(gate) * up).astype(BF16)
             return carry
 
-        lax.fori_loop(0, 4, inner, 0)
+        lax.fori_loop(0, 4, inner, 0, unroll=2)
 
         def down(n, carry):
             result = dot(inner_s[:, 0:512], wd_s[0, :, lanes(n, 512)])
@@ -396,7 +396,7 @@
             e_out[c * PER : c * PER + PER, :, lanes(n, 512)] = result.reshape(PER, CAP, 512).astype(BF16)
             return carry
 
-        lax.fori_loop(0, 4, down, 0)
+        lax.fori_loop(0, 4, down, 0, unroll=2)
         for i in range(max(1, c * PER), c * PER + PER):
             pltpu.make_async_remote_copy(
                 e_out.at[i], ret_s.at[i], r_send, r_recv.at[c],
@@ -414,7 +414,7 @@
             acc_s[:, lanes(n, 512)] += parts[:ROWS] + parts[ROWS:]
             return carry
 
-        lax.fori_loop(0, 4, combine, 0)
+        lax.fori_loop(0, 4, combine, 0, unroll=True)
 
     def total_of(n, total):
         return total + jnp.sum(acc_s[:, lanes(n, 512)], axis=1, keepdims=True)

time: 83.9 us -> 81.3 us (0.969)
  Pallas kernels: 81.8 us -> 79.2 us
    pallas_call x1, Pallas kernels: 81.8 us -> 79.2 us  [per_device(): pl.pallas_call(layer_kernel, name='layer', out_shape=jax.ShapeDtypeStruct...]
where the time goes in v3:
time: 81.3 us; the launch traced here: 81 us
  Pallas kernels  79.2 us (97%)
  local copies, waits for them, and re-layouts  1.88 us (2%)
    pallas_call x1, Pallas kernels, per_device(): pl.pallas_call(layer_kernel, name='layer', out_shape=jax.ShapeDtypeStruct...  79.2 us
    unnamed x1, local copies, waits for them, and re-layouts  1.88 us

profile of v3, /device:TPU:1, one launch (start us, length us, event | category | flops | bytes accessed | tf_op | source)
XLA Modules:
  0.0 81.0 jit_solution(7676217260092484186)
XLA Ops:
  0.0 79.2 %layer.1 = bf16[128,2048]{1,0:T(8,128)(2,1)} custom-call(bf16[256,1024]{1,0:T(8,128)(2,1)} %q_hbm.1, bf16[256,1024]{1,0:T(8,128)(2,1)} %k_hbm.1, bf16[256,1024]{1,0:T(8,128)(2,1)} %v_hbm.1, bf16[256,1024]{1,0:T(8,128)(2,1)} %g_hbm.1, bf16[256,1024]{1,0:T(8,128)(2,1)} %a_hbm.1, f32[16,256]{1,0:T(8,128)} %bitcast.6, bf16[128,2048]{1,0:T(8,128)(2,1)} %res_hbm.1, ...), custom_call_target="tpu_custom_call" | custom-call | tf_op jit(solution)/shard_map/layer/pallas_call | solution.py:488
  79.2 1.9 %copy.21 = bf16[128,2048]{1,0:T(8,128)(2,1)} copy(bf16[128,2048]{1,0:T(8,128)(2,1)} %layer.1) | data formatting | bytes 1048576

commit v4 on v3

--- a/solution.py
+++ b/solution.py
@@ -201,7 +201,7 @@
             local_s[rows, lanes(p)] = result
         return carry
 
-    lax.fori_loop(0, PAIRS // 2, local_pair, 0)
+    lax.fori_loop(0, PAIRS // 2, local_pair, 0, unroll=2)
 
     strict = jnp.where(iota((ROWS, ROWS), 0) < iota((ROWS, ROWS), 1), 1.0, 0.0).astype(BF16)
     slot = iota((ROWS, ROWS), 0)
@@ -241,7 +241,7 @@
         sc_out[at] = state.astype(BF16)
         return state * tot_in[at] + st_in[at].astype(F32)
 
-    lax.fori_loop(0, N_SP, scan_step, jnp.zeros((16, 128), F32), unroll=16)
+    lax.fori_loop(0, N_SP, scan_step, jnp.zeros((16, 128), F32), unroll=64)
 
     for s in FAR_FIRST:
         to = shifted(me, s, 1)
@@ -250,7 +250,7 @@
             device_id={"sp": to}, device_id_type=MESH,
         ).start()
     inc_s[me] = sc_out[me]
-    lax.fori_loop(PAIRS // 2, PAIRS, local_pair, 0)
+    lax.fori_loop(PAIRS // 2, PAIRS, local_pair, 0, unroll=2)
     loads[5].wait()
     gain = jnp.concatenate([hgain_ref[...], hgain_ref[...]], axis=1)
 
@@ -411,15 +411,13 @@
             rows = ret_s[c * PER : c * PER + PER, :, lanes(n, 512)]
             rows = rows.astype(F32).reshape(ROWS, 512).astype(BF16)
             parts = dot(comb_s[c], rows)
-            acc_s[:, lanes(n, 512)] += parts[:ROWS] + parts[ROWS:]
-            return carry
-
-        lax.fori_loop(0, 4, combine, 0, unroll=True)
-
-    def total_of(n, total):
-        return total + jnp.sum(acc_s[:, lanes(n, 512)], axis=1, keepdims=True)
-
-    norm_to(out_ref, fgain_ref, lax.fori_loop(0, 4, total_of, jnp.zeros((ROWS, 1), F32), unroll=True))
+            sums = acc_s[:, lanes(n, 512)] + (parts[:ROWS] + parts[ROWS:])
+            acc_s[:, lanes(n, 512)] = sums
+            return carry + jnp.sum(sums, axis=1, keepdims=True) if c == CHUNKS - 1 else carry
+
+        row_sums = lax.fori_loop(0, 4, combine, jnp.zeros((ROWS, 1), F32), unroll=True)
+
+    norm_to(out_ref, fgain_ref, row_sums)
 
     drain(st_in, N_SP - 1, st_send, st_recv).wait_send()
     drain(tot_in, N_SP - 1, tt_send, tt_recv).wait_send()

time: 81.3 us -> 81.3 us (level)
  no operation moved by 1% of the time
where the time goes in v4:
time: 81.3 us; the launch traced here: 81.1 us
  Pallas kernels  79.2 us (97%)
  local copies, waits for them, and re-layouts  1.88 us (2%)
    pallas_call x1, Pallas kernels, per_device(): pl.pallas_call(layer_kernel, name='layer', out_shape=jax.ShapeDtypeStruct...  79.2 us
    unnamed x1, local copies, waits for them, and re-layouts  1.88 us

profile of v4, /device:TPU:1, one launch (start us, length us, event | category | flops | bytes accessed | tf_op | source)
XLA Modules:
  0.0 81.1 jit_solution(11384807029272608059)
XLA Ops:
  0.0 79.2 %layer.1 = bf16[128,2048]{1,0:T(8,128)(2,1)} custom-call(bf16[256,1024]{1,0:T(8,128)(2,1)} %q_hbm.1, bf16[256,1024]{1,0:T(8,128)(2,1)} %k_hbm.1, bf16[256,1024]{1,0:T(8,128)(2,1)} %v_hbm.1, bf16[256,1024]{1,0:T(8,128)(2,1)} %g_hbm.1, bf16[256,1024]{1,0:T(8,128)(2,1)} %a_hbm.1, f32[16,256]{1,0:T(8,128)} %bitcast.6, bf16[128,2048]{1,0:T(8,128)(2,1)} %res_hbm.1, ...), custom_call_target="tpu_custom_call" | custom-call | tf_op jit(solution)/shard_map/layer/pallas_call | solution.py:486
  79.2 1.9 %copy.21 = bf16[128,2048]{1,0:T(8,128)(2,1)} copy(bf16[128,2048]{1,0:T(8,128)(2,1)} %layer.1) | data formatting | bytes 1048576
